TPU v7x, 512 devices: a whole 4x4x16 slice. The times are simulated.
512 devices in a mesh: ep: 32 (over z, core), tp: 16 (over y, x).
Axes of the slice: x: 4, y: 4, z: 16, core: 2. Of those that a mesh axis runs over, the one named last changes fastest.
Arguments:
- query_rows: bfloat16 [12288, 2048], P('ep', 'tp'), may hold values from -6 to 6
- key_rows: bfloat16 [12288, 2048], P('ep', 'tp'), may hold values from -6 to 6
- value_rows: bfloat16 [12288, 2048], P('ep', 'tp'), may hold values from -6 to 6
- second_scale: float32 [16], P('tp'), may hold values from 0.3 to 0.8
- head_gain: float32 [128], replicated, may hold values from 0.1 to 1.9
- out_weight: bfloat16 [2048, 4096], P(None, 'tp'), may hold values from -0.125 to 0.125
- routed_rows: bfloat16 [4096, 4096], P('ep', 'tp'), may hold values from -6 to 6
- norm_gain: float32 [4096], replicated, may hold values from 0.1 to 1.9
- route_ids: int32 [4096, 2], P('ep'), may hold values from 0 to 31, all different within a row; in each aligned block of 128 rows (0 to 127, 128 to 255, ...) at most 16 rows name the same one
- route_weight: float32 [4096, 2], P('ep'), may hold values from 0.1 to 0.9
- expert_gate: bfloat16 [32, 4096, 2048], P('ep', None, 'tp'), may hold values from -0.09375 to 0.09375
- expert_up: bfloat16 [32, 4096, 2048], P('ep', None, 'tp'), may hold values from -0.09375 to 0.09375
- expert_down: bfloat16 [32, 2048, 4096], P('ep', None, 'tp'), may hold values from -0.125 to 0.125
Outputs:
- mixer_out: bfloat16 [12288, 4096], P('ep', 'tp')
- expert_mix: bfloat16 [4096, 4096], P('ep', 'tp')
Inputs may be any that keep to these rules, and one draw needn't show every extreme that they name: `route_ids`: among the 128 tokens of one index of ep, no expert is named by more than 16 of them, a bound that some block reaches.
All inputs are finite; a program needn't handle non-finite values.
Results may differ from a plain program's by a relative error of at most 0.0085.
Values may be sent and summed in bfloat16 or wider, within the bound.
A program may use at most 64 MiB of HBM per device.

v0:
```python
import jax
import jax.numpy as jnp
from jax import lax
from jax.sharding import PartitionSpec as P

eps = 1e-06
head_factor = 0.8
neg_big = -1e30
key_block_rows = 1024


def side_by_side(arrays, axis, dim, along):
    both = jnp.concatenate(arrays, axis=along)
    result, at, finished = (lax.all_gather(both, axis, axis=dim, tiled=True), 0, [])
    for a in arrays:
        finished.append(lax.slice_in_dim(result, at, at + a.shape[along], axis=along))
        at += a.shape[along]
    return tuple(finished)


def rms_rows(rows_in, gain):
    floats = rows_in.astype(jnp.float32)
    factor = lax.rsqrt(jnp.mean(floats * floats, axis=-1, keepdims=True) + eps)
    return (floats * factor * gain).astype(jnp.bfloat16)


def per_device(
    query_rows,
    key_rows,
    value_rows,
    second_scale,
    head_gain,
    out_weight,
    routed_rows,
    norm_gain,
    route_ids,
    route_weight,
    expert_gate,
    expert_up,
    expert_down,
):
    count_a = query_rows.shape[0]
    per_head = second_scale.shape[0]
    head_dim = query_rows.shape[1] // (2 * per_head)
    value_dim = head_gain.shape[0]
    query_four = query_rows.reshape(count_a, per_head, 2, head_dim)
    query_pos = lax.axis_index("ep") * count_a + jnp.arange(count_a, dtype=jnp.int32)

    def key_block(carry_state, key_part, value_part, block_start):
        key_count = key_part.shape[0]
        key_four = key_part.reshape(key_count, per_head, 2, head_dim)
        value_three = value_part.reshape(key_count, per_head, value_dim)
        scores = jnp.einsum(
            "ihcd,jhcd->ihcj", query_four, key_four, preferred_element_type=jnp.float32
        ) * head_dim ** (-0.5)
        allowed = (
            query_pos[:, None] >= block_start + jnp.arange(key_count, dtype=jnp.int32)[None, :]
        )[:, None, None, :]
        scores = jnp.where(allowed, scores, neg_big)
        old_max, old_sum, old_acc = carry_state
        new_max = jnp.maximum(old_max, jnp.max(scores, axis=-1))
        weights = jnp.where(allowed, jnp.exp(scores - new_max[..., None]), 0.0)
        shrink = jnp.exp(old_max - new_max)
        new_sum = old_sum * shrink + jnp.sum(weights, axis=-1)
        update = jnp.einsum(
            "ihcj,jhe->ihce",
            weights.astype(jnp.bfloat16),
            value_three,
            preferred_element_type=jnp.float32,
        )
        return (new_max, new_sum, old_acc * shrink[..., None] + update)

    start_state = (
        jnp.full((count_a, per_head, 2), neg_big, jnp.float32),
        jnp.zeros((count_a, per_head, 2), jnp.float32),
        jnp.zeros((count_a, per_head, 2, value_dim), jnp.float32),
    )
    key_part, value_part = side_by_side((key_rows, value_rows), "ep", 0, 1)
    key_count = key_part.shape[0]

    def step_block(block_num, inner_state):
        offset_rows = block_num * key_block_rows
        key_slice = lax.dynamic_slice_in_dim(key_part, offset_rows, key_block_rows, 0)
        value_slice = lax.dynamic_slice_in_dim(value_part, offset_rows, key_block_rows, 0)
        return key_block(inner_state, key_slice, value_slice, offset_rows)

    run_max, run_sum, run_acc = lax.fori_loop(
        0, key_count // key_block_rows, step_block, start_state
    )
    maps_both = run_acc / run_sum[..., None]
    mixed_maps = maps_both[:, :, 0] - second_scale[None, :, None] * maps_both[:, :, 1]
    mean_sq = jnp.mean(mixed_maps * mixed_maps, axis=-1, keepdims=True)
    head_out = (
        (mixed_maps * lax.rsqrt(mean_sq + eps) * head_gain * head_factor)
        .astype(jnp.bfloat16)
        .reshape(count_a, per_head * value_dim)
    )
    count_b = routed_rows.shape[0]
    route_count = route_ids.shape[1]
    experts_here = expert_gate.shape[0]
    ep_devices = lax.axis_size("ep")
    expert_total = experts_here * ep_devices
    capacity = 2 * count_b * route_count // expert_total
    flat_expert = route_ids.reshape(-1)
    chosen = (flat_expert[:, None] == jnp.arange(expert_total, dtype=jnp.int32)[None, :]).astype(
        jnp.int32
    )
    ranks = jnp.sum((jnp.cumsum(chosen, axis=0) - 1) * chosen, axis=1)
    slot_of = flat_expert * capacity + ranks
    token_of = jnp.arange(count_b * route_count, dtype=jnp.int32) // route_count
    slot_token = jnp.full((expert_total * capacity,), count_b, jnp.int32).at[slot_of].set(token_of)
    padded = jnp.concatenate(
        [routed_rows, jnp.zeros((1, routed_rows.shape[1]), jnp.bfloat16)], axis=0
    )
    outgoing = padded[slot_token].reshape(ep_devices, experts_here, capacity, routed_rows.shape[1])
    column_parts = lax.all_to_all(outgoing, "ep", split_axis=0, concat_axis=0, tiled=True)
    arrived = rms_rows(lax.all_gather(column_parts, "tp", axis=3, tiled=True), norm_gain)
    gate_val = jnp.einsum(
        "sxcd,xdf->sxcf", arrived, expert_gate, preferred_element_type=jnp.float32
    )
    up_val = jnp.einsum("sxcd,xdf->sxcf", arrived, expert_up, preferred_element_type=jnp.float32)
    hidden = (jax.nn.silu(gate_val) * up_val).astype(jnp.bfloat16)
    weight_rows = out_weight
    attn_total = jnp.dot(
        lax.all_gather(
            head_out.reshape(1, 1, count_a, head_out.shape[1]), "tp", axis=3, tiled=True
        )[0, 0],
        weight_rows,
        preferred_element_type=jnp.float32,
    )
    weight_rows = expert_down
    moe_total = jnp.einsum(
        "sxcf,xfd->sxcd",
        lax.all_gather(hidden, "tp", axis=3, tiled=True),
        weight_rows,
        preferred_element_type=jnp.float32,
    )
    mixer_out = attn_total.astype(jnp.bfloat16)
    returned = lax.all_to_all(
        moe_total.astype(jnp.bfloat16), "ep", split_axis=0, concat_axis=0, tiled=True
    )
    flat_back = returned.reshape(expert_total * capacity, returned.shape[3])
    picked = flat_back[slot_of].astype(jnp.float32).reshape(count_b, route_count, returned.shape[3])
    expert_mix = jnp.sum(picked * route_weight[:, :, None], axis=1).astype(jnp.bfloat16)
    return (mixer_out, expert_mix)


def solution(mesh):
    placed = (
        P("ep", "tp"),
        P("ep", "tp"),
        P("ep", "tp"),
        P("tp"),
        P(),
        P(None, "tp"),
        P("ep", "tp"),
        P(),
        P("ep", None),
        P("ep", None),
        P("ep", None, "tp"),
        P("ep", None, "tp"),
        P("ep", None, "tp"),
    )
    return jax.shard_map(
        per_device,
        mesh=mesh,
        in_specs=placed,
        out_specs=(P("ep", "tp"), P("ep", "tp")),
        check_vma=False,
    )
```

profile of v0, /device:TPU:32, one launch (start us, length us, event | category | flops | bytes accessed | tf_op | source)
XLA Modules:
  0.0 361.6 jit_solution(12429718926275836795)
XLA Ops:
  7.3 0.9 copy.34
  10.3 1.4 scatter_custom_fusion
  12.6 1.9 gather_fusion
  14.6 36.4 %all_to_all.10 = bf16[32,1,16,256]{3,2,1,0:T(8,128)(2,1)} all-to-all(bf16[32,1,16,256]{3,2,1,0:T(8,128)(2,1)S(1)} %bitcast.173), channel_id=1, replica_groups=mesh['ep'=32,'tp'=16] {'ep'}, dimensions={0} | all-to-all | bytes 524288 | tf_op jit(solution)/shard_map/all_to_all | solution.py:116
  52.9 63.2 %all-gather.9.cloned.1.call-done = bf16[32,1,16,4096]{3,2,1,0:T(8,128)(2,1)} async-done(((bf16[32,1,16,256]{3,2,1,0:T(8,128)(2,1)}), bf16[32,1,16,4096]{3,2,1,0:T(8,128)(2,1)}) %all-gather.9.cloned.1.call-update) | async-done | bytes 4194320 | tf_op jit(solution)/shard_map/all_gather | solution.py:117
  116.0 3.2 fusion.24
  119.5 1.3 fusion.42
  120.8 1.9 fusion.54
  122.8 71.9 %all-gather.5.cloned.1.call-done = bf16[12288,256]{0,1:T(8,128)(2,1)} async-done(((bf16[384,256]{0,1:T(8,128)(2,1)}), bf16[12288,256]{0,1:T(8,128)(2,1)}) %all-gather.5.cloned.1.call-update) | async-done | bytes 6291472 | tf_op jit(solution)/shard_map/all_gather | solution.py:14
  194.7 6.2 %fusion.69 = (bf16[12288,128]{0,1:T(8,128)(2,1)}, bf16[12288,128]{0,1:T(8,128)(2,1)}) fusion(bf16[12288,256]{0,1:T(8,128)(2,1)} %all-gather.5.cloned.1.call-done), kind=kLoop, calls=%fused_computation.86 | loop fusion | bytes 12582912 | tf_op jit(solution)/shard_map/slice | solution.py:16
  200.9 94.7 %while.18 = (s32[]{:T(128)}, f32[384,1,2]{0,2,1:T(2,128)S(1)}, f32[384,1,2]{0,2,1:T(2,128)S(1)}, f32[384,1,2,128]{0,3,2,1:T(8,128)S(1)}, bf16[12288,128]{0,1:T(8...) while((s32[]{:T(128)}, f32[384,1,2]{0,2,1:T(2,128)S(1)}, ...), condition=%wide.region_3.4_spmd.clone, body=%wide.region_0.3_spmd.clone.sunk | while | flops 312907648 | bytes 25586904 | solution.py:87
  200.9 1.0 constant_dynamic-slice_fusion.2
  202.2 2.4 fusion.82
  204.6 3.2 fusion.85
  207.9 0.9 fusion.84
  208.8 1.0 constant_dynamic-slice_fusion.2
  210.1 2.4 fusion.82
  212.5 3.2 fusion.85
  215.8 0.9 fusion.84
  216.7 1.0 constant_dynamic-slice_fusion.2
  218.0 2.4 fusion.82
  220.4 3.2 fusion.85
  223.7 0.9 fusion.84
  224.6 1.0 constant_dynamic-slice_fusion.2
  225.8 2.4 fusion.82
  228.3 3.2 fusion.85
  231.6 0.9 fusion.84
  232.5 1.0 constant_dynamic-slice_fusion.2
  233.7 2.4 fusion.82
  236.2 3.2 fusion.85
  239.4 0.9 fusion.84
  240.3 1.0 constant_dynamic-slice_fusion.2
  241.6 2.4 fusion.82
  244.1 3.2 fusion.85
  247.3 0.9 fusion.84
  248.2 1.0 constant_dynamic-slice_fusion.2
  249.5 2.4 fusion.82
  252.0 3.3 fusion.85
  255.3 0.9 fusion.84
  256.2 1.0 constant_dynamic-slice_fusion.2
  257.5 2.4 fusion.82
  259.9 3.2 fusion.85
  263.2 0.9 fusion.84
  264.1 1.0 constant_dynamic-slice_fusion.2
  265.3 2.4 fusion.82
  267.8 3.2 fusion.85
  271.0 0.9 fusion.84
  271.9 1.0 constant_dynamic-slice_fusion.2
  273.2 2.4 fusion.82
  275.7 3.2 fusion.85
  278.9 0.9 fusion.84
  279.8 1.0 constant_dynamic-slice_fusion.2
  281.1 2.4 fusion.82
  283.6 3.2 fusion.85
  287.7 1.0 constant_dynamic-slice_fusion.2
  289.0 2.4 fusion.82
  291.5 3.2 fusion.85
  296.5 3.1 fusion.48
  299.6 8.2 %all-to-all-start.1 = ((bf16[32,1,16,256]{3,2,1,0:T(8,128)(2,1)}), bf16[32,1,16,256]{3,2,1,0:T(8,128)(2,1)S(1)}, u32[]{:S(2)}, u32[]{:S(2)}) async-start(bf16[32,1,16,256]{3,2,1,0:T(8,128)(2,1)} %fusion.48), calls=%async_computation.1 | async-start | bytes 524288 | tf_op jit(solution)/shard_map/all_to_all | solution.py:139
  308.0 20.8 %all-to-all-done.1 = bf16[32,1,16,256]{3,2,1,0:T(8,128)(2,1)S(1)} async-done(((bf16[32,1,16,256]{3,2,1,0:T(8,128)(2,1)}), bf16[32,1,16,256]{3,2,1,0:T(8,128)(2,1)S(1)}, u32[]{:S(2)}, u32[]{:S(2)}) %all-to-all-start.1) | async-done | bytes 262176 | tf_op jit(solution)/shard_map/all_to_all | solution.py:139
  328.8 1.2 gather_fusion.1
  330.1 1.0 multiply_reduce_fusion
  331.1 21.2 %all-gather.7.cloned.1.call-done = bf16[1,1,384,2048]{2,3,1,0:T(8,128)(2,1)} async-done(((bf16[1,1,384,128]{2,3,1,0:T(8,128)(2,1)}), bf16[1,1,384,2048]{2,3,1,0:T(8,128)(2,1)}) %all-gather.7.cloned.1.call-update) | async-done | bytes 1572880 | tf_op jit(solution)/shard_map/all_gather | solution.py:125
  352.4 2.7 fusion.39
  (160 shorter events, 11.2 us)
Async XLA Ops:
  7.2 289.4 %copy-start = (bf16[1,2048,256]{2,1,0:T(8,128)(2,1)S(1)}, bf16[1,2048,256]{2,1,0:T(8,128)(2,1)}, u32[]{:S(2)}) copy-start(bf16[1,2048,256]{2,1,0:T(8,128)(2,1)} %param.27) | copy-start | bytes 3145732
  7.2 43.8 %copy-start.4 = (bf16[384,128]{1,0:T(8,128)(2,1)S(1)}, bf16[384,128]{1,0:T(8,128)(2,1)}, u32[]{:S(2)}) copy-start(bf16[384,128]{1,0:T(8,128)(2,1)} %param.16) | copy-start | bytes 294916
  7.2 43.9 %copy-start.5 = (bf16[384,128]{1,0:T(8,128)(2,1)S(1)}, bf16[384,128]{1,0:T(8,128)(2,1)}, u32[]{:S(2)}) copy-start(bf16[384,128]{1,0:T(8,128)(2,1)} %param.17) | copy-start | bytes 294916
  7.2 44.9 %copy-start.6 = (bf16[384,128]{1,0:T(8,128)(2,1)S(1)}, bf16[384,128]{1,0:T(8,128)(2,1)}, u32[]{:S(2)}) copy-start(bf16[384,128]{1,0:T(8,128)(2,1)} %param.15) | copy-start | bytes 294916
  7.2 108.8 %all-gather.9.cloned.1.call-start = ((), (), s32[]{:S(2)}) async-start(), calls=%async_computation.4 | async-start | bytes 4456448 | tf_op jit(solution)/shard_map/all_gather | solution.py:117
  14.5 104.7 %copy-start.9 = (bf16[1,4096,128]{2,1,0:T(8,128)(2,1)S(1)}, bf16[1,4096,128]{2,1,0:T(8,128)(2,1)}, u32[]{:S(2)}) copy-start(bf16[1,4096,128]{2,1,0:T(8,128)(2,1)} %param.25) | copy-start | bytes 3145732
  14.5 104.7 %copy-start.11 = (f32[4096]{0:T(1024)S(1)}, f32[4096]{0:T(1024)}, u32[]{:S(2)}) copy-start(f32[4096]{0:T(1024)} %param.22) | copy-start | bytes 49156
  50.9 143.8 %all-gather.5.cloned.1.call-start = ((), (), s32[]{:S(2)}) async-start(), calls=%async_computation.2 | async-start | bytes 6488064 | tf_op jit(solution)/shard_map/all_gather | solution.py:14
  52.0 244.5 %all-gather.11.cloned.1.call-start = ((), (), s32[]{:S(2)}) async-start(), calls=%async_computation.5 | async-start | bytes 2228224 | tf_op jit(solution)/shard_map/all_gather | solution.py:134
  116.0 3.4 copy-start.2
  119.5 1.3 copy-start.10
  122.8 229.6 %all-gather.7.cloned.1.call-start = ((), (), s32[]{:S(2)}) async-start(), calls=%async_computation.3 | async-start | bytes 1671168 | tf_op jit(solution)/shard_map/all_gather | solution.py:125
  200.9 94.8 %copy-start.8 = (f32[128]{0:T(128)S(1)}, f32[128]{0:T(128)}, u32[]{:S(2)}) copy-start(f32[128]{0:T(128)} %param.19) | copy-start | bytes 1540
  204.6 3.3 copy-start.1
  212.5 3.3 copy-start.1
  220.4 3.3 copy-start.1
  228.3 3.3 copy-start.1
  236.2 3.3 copy-start.1
  244.1 3.3 copy-start.1
  252.0 3.3 copy-start.1
  259.9 3.3 copy-start.1
  267.8 3.3 copy-start.1
  275.7 3.3 copy-start.1
  283.6 3.3 copy-start.1
  291.5 3.3 copy-start.1
  295.6 12.3 %copy-start.7 = (f32[128,2]{0,1:T(2,128)S(1)}, f32[128,2]{0,1:T(2,128)}, u32[]{:S(2)}) copy-start(f32[128,2]{0,1:T(2,128)} %param.24) | copy-start | bytes 3076
  296.5 55.9 %copy-start.3 = (bf16[2048,256]{1,0:T(8,128)(2,1)S(1)}, bf16[2048,256]{1,0:T(8,128)(2,1)}, u32[]{:S(2)}) copy-start(bf16[2048,256]{1,0:T(8,128)(2,1)} %param.20) | copy-start | bytes 3145732
  299.6 29.2 %all-to-all-start.1 = ((bf16[32,1,16,256]{3,2,1,0:T(8,128)(2,1)}), bf16[32,1,16,256]{3,2,1,0:T(8,128)(2,1)S(1)}, u32[]{:S(2)}, u32[]{:S(2)}) async-start(bf16[32,1,16,256]{3,2,1,0:T(8,128)(2,1)} %fusion.48), calls=%async_computation.1 | async-start | bytes 524288 | tf_op jit(solution)/shard_map/all_to_all | solution.py:139
Sparse Core Ops, SparseCore 0:
  51.1 64.9 all-gather.8
  118.7 75.9 all-gather.4
  197.7 59.0 all-gather.10
  296.6 55.7 all-gather.6
where the time goes:
time: 362 us
  waiting for transfers between devices  177 us (49%)
  matrix products  77 us (21%)
  blocking collectives  36.4 us (10%)
  local copies, waits for them, and re-layouts  25.7 us (7%)
  other arithmetic  21.3 us (6%)
  between operations  14.7 us (4%)
  starting transfers between devices  8.4 us (2%)
    all_gather x1, waiting for transfers between devices, side_by_side(): lax.all_gather(both, axis, axis=dim, tiled=True)  71.9 us
    all_gather x1, waiting for transfers between devices, per_device(): lax.all_gather(column_parts, 'tp', axis=3, tiled=True)  63.2 us
    dot_general x12, matrix products, key_block(): jnp.einsum('ihcj,jhe->ihce', weights.astype(jnp.bfloat16), value_three, p...  38.8 us
    all_to_all x1, blocking collectives, per_device(): lax.all_to_all(outgoing, 'ep', split_axis=0, concat_axis=0, tiled=True)  36.4 us
    dot_general x12, matrix products, key_block(): jnp.einsum('ihcd,jhcd->ihcj', query_four, key_four, preferred_element_typ...  29.1 us
    all_gather x1, waiting for transfers between devices, per_device(): lax.all_gather(head_out.reshape(1, 1, count_a, head_out.shape[1]), 'tp',...  21.2 us
    all_to_all x1, waiting for transfers between devices, per_device(): lax.all_to_all(moe_total.astype(jnp.bfloat16), 'ep', split_axis=0, concat...  20.8 us
    dynamic_slice x12, local copies, waits for them, and re-layouts, step_block(): lax.dynamic_slice_in_dim(key_part, offset_rows, key_block_rows, 0)  11.7 us
  transfers between devices with their start and end apart: 5, of which 4 were waited for; matrix products, arithmetic and copies ran while one was open for 31% of the time, Pallas kernels for 0%

commit v1 on v0

--- a/solution.py
+++ b/solution.py
@@ -1,3 +1,4 @@
+import functools
 import jax
 import jax.numpy as jnp
 from jax import lax
@@ -7,6 +8,33 @@
 head_factor = 0.8
 neg_big = -1e30
 key_block_rows = 1024
+
+
+def turn_stacks_all_up(field_in, row_axis, out_dim):
+    small, front, local_next = (
+        lax.axis_size(row_axis),
+        lax.axis_index(row_axis),
+        field_in.shape[out_dim],
+    )
+    value_now, current_block = (field_in, 1)
+    while current_block < small:
+        value_now = jnp.concatenate(
+            [
+                value_now,
+                lax.ppermute(
+                    value_now,
+                    row_axis,
+                    tuple(((i0, (i0 - current_block) % small) for i0 in range(small))),
+                ),
+            ],
+            out_dim,
+        )
+        current_block = 2 * current_block
+    tile_out = jnp.roll(value_now, front * local_next, out_dim)
+    return tile_out
+
+
+set_the_face = functools.partial(turn_stacks_all_up, row_axis="tp", out_dim=3)
 
 
 def side_by_side(arrays, axis, dim, along):
@@ -114,7 +142,7 @@
     )
     outgoing = padded[slot_token].reshape(ep_devices, experts_here, capacity, routed_rows.shape[1])
     column_parts = lax.all_to_all(outgoing, "ep", split_axis=0, concat_axis=0, tiled=True)
-    arrived = rms_rows(lax.all_gather(column_parts, "tp", axis=3, tiled=True), norm_gain)
+    arrived = rms_rows(set_the_face(column_parts), norm_gain)
     gate_val = jnp.einsum(
         "sxcd,xdf->sxcf", arrived, expert_gate, preferred_element_type=jnp.float32
     )

time: 362 us -> 338 us (0.934)
  waiting for transfers between devices: 177 us -> 121 us
  starting transfers between devices: 8.4 us -> 30.2 us
  local copies, waits for them, and re-layouts: 25.7 us -> 32.8 us
    ppermute x0 -> x4, waiting for transfers between devices: none -> 76 us  [turn_stacks_all_up(): lax.ppermute(value_now, row_axis, tuple(((i0, (i0 - current_block) % smal...]
    all_gather x1, waiting for transfers between devices: 71.9 us -> 0.02 us  [side_by_side(): lax.all_gather(both, axis, axis=dim, tiled=True)]
    all_gather x1 -> x0, waiting for transfers between devices: 63.2 us -> none  [per_device(): lax.all_gather(column_parts, 'tp', axis=3, tiled=True)]
    ppermute x0 -> x4, starting transfers between devices: none -> 17.8 us  [turn_stacks_all_up(): lax.ppermute(value_now, row_axis, tuple(((i0, (i0 - current_block) % smal...]
    unnamed x27 -> x30, local copies, waits for them, and re-layouts: 1.6 us -> 6.83 us
    all_to_all x1, starting transfers between devices: 8.23 us -> 12.2 us  [per_device(): lax.all_to_all(moe_total.astype(jnp.bfloat16), 'ep', split_axis=0, concat...]
  transfers between devices with their start and end apart: 5 -> 8, of which waited for: 4 -> 6; matrix products, arithmetic and copies ran while one was open for 31% -> 37% of each run, Pallas kernels for 0% -> 0%
where the time goes in v1:
time: 338 us; the launch traced here: 337 us
  waiting for transfers between devices  121 us (36%)
  matrix products  77.1 us (23%)
  blocking collectives  39.7 us (12%)
  local copies, waits for them, and re-layouts  32.8 us (10%)
  starting transfers between devices  30.2 us (9%)
  other arithmetic  20.7 us (6%)
  between operations  14.8 us (4%)
    ppermute x4, waiting for transfers between devices, turn_stacks_all_up(): lax.ppermute(value_now, row_axis, tuple(((i0, (i0 - current_block) % smal...  76 us
    all_to_all x1, blocking collectives, per_device(): lax.all_to_all(outgoing, 'ep', split_axis=0, concat_axis=0, tiled=True)  39.7 us
    dot_general x12, matrix products, key_block(): jnp.einsum('ihcj,jhe->ihce', weights.astype(jnp.bfloat16), value_three, p...  38.9 us
    dot_general x12, matrix products, key_block(): jnp.einsum('ihcd,jhcd->ihcj', query_four, key_four, preferred_element_typ...  29.3 us
    all_gather x1, waiting for transfers between devices, per_device(): lax.all_gather(head_out.reshape(1, 1, count_a, head_out.shape[1]), 'tp',...  24.3 us
    all_to_all x1, waiting for transfers between devices, per_device(): lax.all_to_all(moe_total.astype(jnp.bfloat16), 'ep', split_axis=0, concat...  20.8 us
    ppermute x4, starting transfers between devices, turn_stacks_all_up(): lax.ppermute(value_now, row_axis, tuple(((i0, (i0 - current_block) % smal...  17.8 us
    all_to_all x1, starting transfers between devices, per_device(): lax.all_to_all(moe_total.astype(jnp.bfloat16), 'ep', split_axis=0, concat...  12.2 us
  transfers between devices with their start and end apart: 8, of which 6 were waited for; matrix products, arithmetic and copies ran while one was open for 37% of the time, Pallas kernels for 0%

profile of v1, /device:TPU:32, one launch (start us, length us, event | category | flops | bytes accessed | tf_op | source)
XLA Modules:
  0.0 337.4 jit_solution(11104766812872295247)
XLA Ops:
  7.2 1.1 copy.30
  8.3 1.0 copy.31
  13.9 1.4 scatter_custom_fusion
  15.3 2.0 gather_fusion
  17.3 39.7 %all_to_all.10 = bf16[32,1,16,256]{3,2,1,0:T(8,128)(2,1)S(1)} all-to-all(bf16[32,1,16,256]{3,2,1,0:T(8,128)(2,1)S(1)} %bitcast.171), channel_id=1, replica_groups=mesh['ep'=32,'tp'=16] {'ep'}, dimensions={0} | all-to-all | bytes 524288 | tf_op jit(solution)/shard_map/all_to_all | solution.py:144
  57.0 6.8 %collective-permute-start = (bf16[32,1,16,256]{3,2,1,0:T(8,128)(2,1)S(1)}, bf16[32,1,16,256]{3,2,1,0:T(8,128)(2,1)S(1)}, u32[]{:S(2)}, u32[]{:S(2)}) collective-permute-start(bf16[32,1,16,256]{3,2,1,0:T(8,128)(2,1)S(1)} %all_to_all.10), channel_id=1, source_target_pairs={{0,15},{1,0},{2,1},{3,2},{4,3},{5,4},{6,5},{7,6},{8,7},{9,8},{10,9... | collective-permute-start | bytes 786440 | tf_op jit(solution)/shard_map/ppermute | solution.py:24
  63.8 4.1 %collective-permute-done = bf16[32,1,16,256]{3,2,1,0:T(8,128)(2,1)S(1)} collective-permute-done((bf16[32,1,16,256]{3,2,1,0:T(8,128)(2,1)S(1)}, bf16[32,1,16,256]{3,2,1,0:T(8,128)(2,1)S(1)}, u32[]{:S(2)}, u32[]{:S(2)}) %collective-permute-start) | collective-permute-done | bytes 262176 | tf_op jit(solution)/shard_map/ppermute | solution.py:24
  68.0 4.7 %collective-permute-start.1 = (bf16[32,1,16,512]{3,2,1,0:T(8,128)(2,1)S(1)}, bf16[32,1,16,512]{3,2,1,0:T(8,128)(2,1)S(1)}, u32[]{:S(2)}, u32[]{:S(2)}) collective-permute-start(bf16[32,1,16,512]{3,2,1,0:T(8,128)(2,1)S(1)} %pad_maximum_fusion.2), channel_id=1, source_target_pairs={{0,14},{1,15},{2,0},{3,1},{4,2},{5,3},{6,4},{7,5},{8,6},{9,7},{10,... | collective-permute-start | bytes 1572872 | tf_op jit(solution)/shard_map/ppermute | solution.py:24
  72.7 10.1 %collective-permute-done.1 = bf16[32,1,16,512]{3,2,1,0:T(8,128)(2,1)S(1)} collective-permute-done((bf16[32,1,16,512]{3,2,1,0:T(8,128)(2,1)S(1)}, bf16[32,1,16,512]{3,2,1,0:T(8,128)(2,1)S(1)}, u32[]{:S(2)}, u32[]{:S(2)}) %collective-permute-start.1) | collective-permute-done | bytes 524320 | tf_op jit(solution)/shard_map/ppermute | solution.py:24
  82.9 2.9 collective-permute-start.2
  85.8 20.8 %collective-permute-done.2 = bf16[32,1,16,1024]{3,2,1,0:T(8,128)(2,1)S(1)} collective-permute-done((bf16[32,1,16,1024]{3,2,1,0:T(8,128)(2,1)S(1)}, bf16[32,1,16,1024]{3,2,1,0:T(8,128)(2,1)S(1)}, u32[]{:S(2)}, u32[]{:S(2)}) %collective-permute-start.2) | collective-permute-done | bytes 1048608 | tf_op jit(solution)/shard_map/ppermute | solution.py:24
  106.6 1.6 pad_maximum_fusion
  108.1 3.4 %collective-permute-start.3 = (bf16[32,1,16,2048]{3,2,1,0:T(8,128)(2,1)}, bf16[32,1,16,2048]{3,2,1,0:T(8,128)(2,1)}, u32[]{:S(2)}, u32[]{:S(2)}) collective-permute-start(bf16[32,1,16,2048]{3,2,1,0:T(8,128)(2,1)} %pad_maximum_fusion), channel_id=1, source_target_pairs={{0,8},{1,9},{2,10},{3,11},{4,12},{5,13},{6,14},{7,15},{8,0},{9,1},... | collective-permute-start | bytes 6291464 | tf_op jit(solution)/shard_map/ppermute | solution.py:24
  111.6 1.6 copy.32
  114.1 41.1 %collective-permute-done.3 = bf16[32,1,16,2048]{3,2,1,0:T(8,128)(2,1)} collective-permute-done((bf16[32,1,16,2048]{3,2,1,0:T(8,128)(2,1)}, bf16[32,1,16,2048]{3,2,1,0:T(8,128)(2,1)}, u32[]{:S(2)}, u32[]{:S(2)}) %collective-permute-start.3) | collective-permute-done | bytes 2097184 | tf_op jit(solution)/shard_map/ppermute | solution.py:24
  155.2 1.7 constant_dynamic-update-slice_fusion.5
  157.2 1.8 constant_dynamic-update-slice_fusion
  160.0 1.3 fusion.42
  161.3 1.9 multiply_convert_fusion
  163.5 6.2 %fusion.69 = (bf16[12288,128]{0,1:T(8,128)(2,1)}, bf16[12288,128]{0,1:T(8,128)(2,1)}) fusion(bf16[12288,256]{0,1:T(8,128)(2,1)} %all-gather.4.cloned.1.call-done), kind=kLoop, calls=%fused_computation.100 | loop fusion | bytes 12582912 | tf_op jit(solution)/shard_map/slice | solution.py:44
  169.7 94.8 %while.18 = (s32[]{:T(128)}, f32[384,1,2]{0,2,1:T(2,128)S(1)}, f32[384,1,2]{0,2,1:T(2,128)S(1)}, f32[384,1,2,128]{0,3,2,1:T(8,128)S(1)}, bf16[12288,128]{0,1:T(8...) while((s32[]{:T(128)}, f32[384,1,2]{0,2,1:T(2,128)S(1)}, ...), condition=%wide.region_3.4_spmd.clone, body=%wide.region_0.3_spmd.clone.sunk | while | flops 312907648 | bytes 25586904 | solution.py:115
  169.7 1.0 constant_dynamic-slice_fusion.2
  171.0 2.4 fusion.82
  173.4 3.2 fusion.85
  177.6 1.0 constant_dynamic-slice_fusion.2
  178.9 2.4 fusion.82
  181.3 3.2 fusion.85
  185.5 1.0 constant_dynamic-slice_fusion.2
  186.8 2.4 fusion.82
  189.2 3.3 fusion.85
  193.4 1.0 constant_dynamic-slice_fusion.2
  194.7 2.4 fusion.82
  197.2 3.2 fusion.85
  201.3 1.0 constant_dynamic-slice_fusion.2
  202.6 2.4 fusion.82
  205.1 3.2 fusion.85
  209.2 1.0 constant_dynamic-slice_fusion.2
  210.5 2.4 fusion.82
  212.9 3.3 fusion.85
  217.1 1.0 constant_dynamic-slice_fusion.2
  218.4 2.4 fusion.82
  220.9 3.2 fusion.85
  225.0 1.0 constant_dynamic-slice_fusion.2
  226.3 2.4 fusion.82
  228.8 3.2 fusion.85
  232.9 1.0 constant_dynamic-slice_fusion.2
  234.2 2.4 fusion.82
  236.7 3.2 fusion.85
  240.8 1.0 constant_dynamic-slice_fusion.2
  242.1 2.4 fusion.82
  244.6 3.2 fusion.85
  248.7 1.0 constant_dynamic-slice_fusion.2
  250.0 2.4 fusion.82
  252.5 3.2 fusion.85
  256.6 1.0 constant_dynamic-slice_fusion.2
  257.9 2.4 fusion.82
  260.4 3.2 fusion.85
  265.4 3.0 fusion.48
  268.4 12.2 %all-to-all-start.1 = ((bf16[32,1,16,256]{3,2,1,0:T(8,128)(2,1)}), bf16[32,1,16,256]{3,2,1,0:T(8,128)(2,1)S(1)}, u32[]{:S(2)}, u32[]{:S(2)}) async-start(bf16[32,1,16,256]{3,2,1,0:T(8,128)(2,1)} %fusion.48), calls=%async_computation.1 | async-start | bytes 524288 | tf_op jit(solution)/shard_map/all_to_all | solution.py:167
  280.7 20.8 %all-to-all-done.1 = bf16[32,1,16,256]{3,2,1,0:T(8,128)(2,1)S(1)} async-done(((bf16[32,1,16,256]{3,2,1,0:T(8,128)(2,1)}), bf16[32,1,16,256]{3,2,1,0:T(8,128)(2,1)S(1)}, u32[]{:S(2)}, u32[]{:S(2)}) %all-to-all-start.1) | async-done | bytes 262176 | tf_op jit(solution)/shard_map/all_to_all | solution.py:167
  301.6 1.2 gather_fusion.1
  302.9 1.0 multiply_reduce_fusion
  303.9 24.3 %all-gather.6.cloned.1.call-done = bf16[1,1,384,2048]{2,3,1,0:T(8,128)(2,1)} async-done(((bf16[1,1,384,128]{2,3,1,0:T(8,128)(2,1)}), bf16[1,1,384,2048]{2,3,1,0:T(8,128)(2,1)}) %all-gather.6.cloned.1.call-update) | async-done | bytes 1572880 | tf_op jit(solution)/shard_map/all_gather | solution.py:153
  328.2 2.7 fusion.39
  (172 shorter events, 21.6 us)
Async XLA Ops:
  7.2 258.3 %copy-start = (bf16[1,2048,256]{2,1,0:T(8,128)(2,1)S(1)}, bf16[1,2048,256]{2,1,0:T(8,128)(2,1)}, u32[]{:S(2)}) copy-start(bf16[1,2048,256]{2,1,0:T(8,128)(2,1)} %param.27) | copy-start | bytes 3145732
  7.2 156.3 %all-gather.4.cloned.1.call-start = ((), (), s32[]{:S(2)}) async-start(), calls=%async_computation.2 | async-start | bytes 6488064 | tf_op jit(solution)/shard_map/all_gather | solution.py:42
  10.1 255.4 %all-gather.8.cloned.1.call-start = ((), (), s32[]{:S(2)}) async-start(), calls=%async_computation.4 | async-start | bytes 2228224 | tf_op jit(solution)/shard_map/all_gather | solution.py:162
  57.0 10.9 %collective-permute-start = (bf16[32,1,16,256]{3,2,1,0:T(8,128)(2,1)S(1)}, bf16[32,1,16,256]{3,2,1,0:T(8,128)(2,1)S(1)}, u32[]{:S(2)}, u32[]{:S(2)}) collective-permute-start(bf16[32,1,16,256]{3,2,1,0:T(8,128)(2,1)S(1)} %all_to_all.10), channel_id=1, source_target_pairs={{0,15},{1,0},{2,1},{3,2},{4,3},{5,4},{6,5},{7,6},{8,7},{9,8},{10,9... | collective-permute-start | bytes 786440 | tf_op jit(solution)/shard_map/ppermute | solution.py:24
  68.0 14.8 %collective-permute-start.1 = (bf16[32,1,16,512]{3,2,1,0:T(8,128)(2,1)S(1)}, bf16[32,1,16,512]{3,2,1,0:T(8,128)(2,1)S(1)}, u32[]{:S(2)}, u32[]{:S(2)}) collective-permute-start(bf16[32,1,16,512]{3,2,1,0:T(8,128)(2,1)S(1)} %pad_maximum_fusion.2), channel_id=1, source_target_pairs={{0,14},{1,15},{2,0},{3,1},{4,2},{5,3},{6,4},{7,5},{8,6},{9,7},{10,... | collective-permute-start | bytes 1572872 | tf_op jit(solution)/shard_map/ppermute | solution.py:24
  82.9 23.6 %collective-permute-start.2 = (bf16[32,1,16,1024]{3,2,1,0:T(8,128)(2,1)S(1)}, bf16[32,1,16,1024]{3,2,1,0:T(8,128)(2,1)S(1)}, u32[]{:S(2)}, u32[]{:S(2)}) collective-permute-start(bf16[32,1,16,1024]{3,2,1,0:T(8,128)(2,1)S(1)} %pad_maximum_fusion.1), channel_id=1, source_target_pairs={{0,12},{1,13},{2,14},{3,15},{4,0},{5,1},{6,2},{7,3},{8,4},{9,5},{1... | collective-permute-start | bytes 3145736 | tf_op jit(solution)/shard_map/ppermute | solution.py:24
  108.1 47.1 %collective-permute-start.3 = (bf16[32,1,16,2048]{3,2,1,0:T(8,128)(2,1)}, bf16[32,1,16,2048]{3,2,1,0:T(8,128)(2,1)}, u32[]{:S(2)}, u32[]{:S(2)}) collective-permute-start(bf16[32,1,16,2048]{3,2,1,0:T(8,128)(2,1)} %pad_maximum_fusion), channel_id=1, source_target_pairs={{0,8},{1,9},{2,10},{3,11},{4,12},{5,13},{6,14},{7,15},{8,0},{9,1},... | collective-permute-start | bytes 6291464 | tf_op jit(solution)/shard_map/ppermute | solution.py:24
  157.2 2.8 copy-start.6
  157.2 2.8 copy-start.8
  160.0 1.3 copy-start.7
  163.3 6.4 %copy-start.3 = (bf16[384,128]{0,1:T(8,128)(2,1)S(1)}, bf16[384,128]{0,1:T(8,128)(2,1)}, u32[]{:S(2)}) copy-start(bf16[384,128]{0,1:T(8,128)(2,1)} %copy.32) | copy-start | bytes 294916
  163.3 164.9 %all-gather.6.cloned.1.call-start = ((), (), s32[]{:S(2)}) async-start(), calls=%async_computation.3 | async-start | bytes 1671168 | tf_op jit(solution)/shard_map/all_gather | solution.py:153
  169.7 94.9 %copy-start.5 = (f32[128]{0:T(128)S(1)}, f32[128]{0:T(128)}, u32[]{:S(2)}) copy-start(f32[128]{0:T(128)} %param.19) | copy-start | bytes 1540
  173.4 3.3 copy-start.1
  181.3 3.3 copy-start.1
  189.2 3.3 copy-start.1
  197.1 3.3 copy-start.1
  205.0 3.3 copy-start.1
  212.9 3.3 copy-start.1
  220.9 3.3 copy-start.1
  228.8 3.3 copy-start.1
  236.7 3.3 copy-start.1
  244.6 3.3 copy-start.1
  252.4 3.3 copy-start.1
  260.3 3.3 copy-start.1
  264.5 16.1 %copy-start.4 = (f32[128,2]{0,1:T(2,128)S(1)}, f32[128,2]{0,1:T(2,128)}, u32[]{:S(2)}) copy-start(f32[128,2]{0,1:T(2,128)} %param.24) | copy-start | bytes 3076
  264.5 63.7 %copy-start.2 = (bf16[2048,256]{1,0:T(8,128)(2,1)S(1)}, bf16[2048,256]{1,0:T(8,128)(2,1)}, u32[]{:S(2)}) copy-start(bf16[2048,256]{1,0:T(8,128)(2,1)} %param.20) | copy-start | bytes 3145732
  268.4 33.1 %all-to-all-start.1 = ((bf16[32,1,16,256]{3,2,1,0:T(8,128)(2,1)}), bf16[32,1,16,256]{3,2,1,0:T(8,128)(2,1)S(1)}, u32[]{:S(2)}, u32[]{:S(2)}) async-start(bf16[32,1,16,256]{3,2,1,0:T(8,128)(2,1)} %fusion.48), calls=%async_computation.1 | async-start | bytes 524288 | tf_op jit(solution)/shard_map/all_to_all | solution.py:167
Sparse Core Ops, SparseCore 0:
  10.6 88.9 all-gather.3
  163.4 65.9 all-gather.7
  265.5 62.6 all-gather.5
